TPU v7x, 32 devices: a whole 2x2x4 slice. The times are simulated.
32 devices in a mesh: grp: 2 (over y), ep: 4 (over z), tp: 4 (over x, core).
Axes of the slice: x: 2, y: 2, z: 4, core: 2. Of those that a mesh axis runs over, the one named last changes fastest.
Arguments:
- queries: bfloat16 [1024, 1024], P(('grp', 'ep'), 'tp'), parts along dimension 0, may hold values from -6 to 6
- keys: bfloat16 [1024, 1024], P(('grp', 'ep'), 'tp'), parts along dimension 0, may hold values from -6 to 6
- values: bfloat16 [1024, 1024], P(('grp', 'ep'), 'tp'), parts along dimension 0, may hold values from -6 to 6
- lambdas: float32 [8], P('tp'), may hold values from 0.3 to 0.8
- head_gain: float32 [128], replicated, may hold values from 0.1 to 1.9
- tokens: bfloat16 [2048, 1536], P(('grp', 'ep')), parts along dimension 0, may hold values from -6 to 6
- route_ids: int32 [2048, 2], P(('grp', 'ep')), parts along dimension 0, may hold values from 0 to 3, all different within a row; in each aligned block of 256 rows (0 to 255, 256 to 511, ...) at most 256 rows name the same one
- route_weights: float32 [2048, 2], P(('grp', 'ep')), parts along dimension 0, may hold values from 0.2 to 1
- moe_gain: float32 [1536], replicated, may hold values from 0.1 to 1.9
- w_gate: bfloat16 [4, 1536, 3072], P('ep', None, 'tp'), may hold values from -0.15625 to 0.15625
- w_up: bfloat16 [4, 1536, 3072], P('ep', None, 'tp'), may hold values from -0.15625 to 0.15625
- w_down: bfloat16 [4, 3072, 1536], P('ep', 'tp'), may hold values from -0.109375 to 0.109375
Outputs:
- heads_out: bfloat16 [1024, 1024], P(('grp', 'ep'), 'tp'), parts along dimension 0
- expert_out: bfloat16 [2048, 1536], P(('grp', 'ep'), 'tp'), parts along dimension 0
There are 2 independent parts, one for each index of `grp`. A program takes and returns all parts, laid end to end along the dimension named above; an argument that names none is the same for every part. Nothing has to cross between parts.
Inputs may be any that keep to these rules, and one draw needn't show every extreme that they name: `route_ids`: each row names 2 different experts. In the 256 rows of one device no expert is named more than 256 times, and in every draw some device names some expert exactly 256 times.
All inputs are finite; a program needn't handle non-finite values.
Results may differ from a plain program's by a relative error of at most 0.015.
Values may be sent and summed in bfloat16 or wider, within the bound.
A program may use at most 64 MiB of HBM per device.

v0:
```python
import jax
import jax.numpy as jnp
from jax import lax
from jax.sharding import PartitionSpec as P


def attend(queries, keys, values, lambdas, head_gain):
    row_count = queries.shape[0]
    head_count = lambdas.shape[0]
    head_dim = queries.shape[1] // (2 * head_count)
    value_dim = values.shape[1] // head_count
    query_parts = queries.reshape(row_count, head_count, 2, head_dim)
    score_scale = head_dim ** (-0.5)
    running = jnp.full((head_count, 2, row_count), -1e30, jnp.float32)
    key_piece = lax.all_gather(keys, "ep", axis=0, tiled=True)
    value_piece = lax.all_gather(values, "ep", axis=0, tiled=True)
    count = key_piece.shape[0]
    key_parts = key_piece.reshape(count, head_count, 2, head_dim)
    value_parts = value_piece.reshape(count, head_count, value_dim)
    scores = (
        jnp.einsum("qhcd,khcd->hcqk", query_parts, key_parts, preferred_element_type=jnp.float32)
        * score_scale
    )
    newest = jnp.maximum(running, jnp.max(scores, axis=-1))
    weights_now = jnp.exp(scores - newest[..., None])
    totals = jnp.sum(weights_now, axis=-1)
    sums = jnp.einsum(
        "hcqk,khe->hcqe",
        weights_now.astype(jnp.bfloat16),
        value_parts,
        preferred_element_type=jnp.float32,
    )
    running, totals, sums = (newest, totals, sums)
    means = sums / totals[..., None]
    mixed = means[:, 0] - lambdas[:, None, None] * means[:, 1]
    scaled = mixed * lax.rsqrt(jnp.mean(mixed * mixed, axis=-1, keepdims=True) + 1e-06) * head_gain
    return (
        jnp.transpose(scaled, (1, 0, 2))
        .reshape(row_count, head_count * value_dim)
        .astype(jnp.bfloat16)
    )


def experts(tokens, route_ids, route_weights, moe_gain, w_gate, w_up, w_down):
    row_count, width = tokens.shape
    top_count = route_ids.shape[1]
    ep_size = lax.axis_size("ep")
    tp_size = lax.axis_size("tp")
    expert_count = w_gate.shape[0] * ep_size
    capacity = 2 * row_count * top_count // expert_count
    token_float = tokens.astype(jnp.float32)
    normed = (
        token_float
        * lax.rsqrt(jnp.mean(token_float * token_float, axis=1, keepdims=True) + 1e-06)
        * moe_gain
    ).astype(jnp.bfloat16)
    flat_ids = route_ids.reshape(-1)
    onehot = (flat_ids[:, None] == jnp.arange(expert_count, dtype=jnp.int32)[None, :]).astype(
        jnp.int32
    )
    earlier = jnp.cumsum(onehot, axis=0) - onehot
    position = jnp.sum(earlier * onehot, axis=1)
    slot_index = flat_ids * capacity + position
    owners = (
        jnp.full((expert_count * capacity,), row_count, jnp.int32)
        .at[slot_index]
        .set(jnp.arange(row_count * top_count, dtype=jnp.int32) // top_count)
    )
    padded = jnp.concatenate([normed, jnp.zeros((1, width), jnp.bfloat16)], axis=0)
    outgoing = padded[owners].reshape(expert_count, capacity, width)
    gate_mat = w_gate[0]
    up_mat = w_up[0]
    down_mat = w_down[0]
    slice_width = width // tp_size
    own_columns = lax.dynamic_slice_in_dim(
        outgoing, lax.axis_index("tp") * slice_width, slice_width, 2
    )
    arrived = lax.all_to_all(own_columns, "ep", split_axis=0, concat_axis=0, tiled=True)
    piece = lax.all_gather(arrived, "tp", axis=2, tiled=True)
    gate = jnp.einsum("scd,df->scf", piece, gate_mat, preferred_element_type=jnp.float32)
    upward = jnp.einsum("scd,df->scf", piece, up_mat, preferred_element_type=jnp.float32)
    hidden = (jax.nn.silu(gate) * upward).astype(jnp.bfloat16)
    flat_hidden = hidden.reshape(-1, hidden.shape[2])
    summed = lax.psum_scatter(
        jnp.einsum("fd,sf->ds", down_mat, flat_hidden, preferred_element_type=jnp.float32).astype(
            jnp.bfloat16
        ),
        "tp",
        scatter_dimension=0,
        tiled=True,
    )
    back = lax.all_to_all(summed, "ep", split_axis=1, concat_axis=1, tiled=True)
    picked = (
        jnp.take(back, slot_index, axis=1).astype(jnp.float32).reshape(-1, row_count, top_count)
    )
    combined = jnp.einsum("drk,rk->rd", picked, route_weights)
    return combined.astype(jnp.bfloat16)


def on_device(
    queries,
    keys,
    values,
    lambdas,
    head_gain,
    tokens,
    route_ids,
    route_weights,
    moe_gain,
    w_gate,
    w_up,
    w_down,
):
    heads_out = attend(queries, keys, values, lambdas, head_gain)
    expert_out = experts(tokens, route_ids, route_weights, moe_gain, w_gate, w_up, w_down)
    return (heads_out, expert_out)


def solution(mesh):
    in_specs = (
        P(("grp", "ep"), "tp"),
        P(("grp", "ep"), "tp"),
        P(("grp", "ep"), "tp"),
        P("tp"),
        P(),
        P(("grp", "ep"), None),
        P(("grp", "ep"), None),
        P(("grp", "ep"), None),
        P(),
        P("ep", None, "tp"),
        P("ep", None, "tp"),
        P("ep", "tp", None),
    )
    out_specs = (P(("grp", "ep"), "tp"), P(("grp", "ep"), "tp"))
    return jax.shard_map(
        on_device, mesh=mesh, in_specs=in_specs, out_specs=out_specs, check_vma=False
    )
```

profile of v0, /device:TPU:0, one launch (start us, length us, event | category | flops | bytes accessed | tf_op | source)
XLA Modules:
  0.0 183.2 jit_solution(15858981580019613275)
XLA Ops:
  7.2 1.0 copy.40
  8.5 0.7 broadcast_multiply_fusion
  9.2 1.2 reduce-window.6
  10.4 0.2 slice_reduce_fusion
  10.6 0.2 reduce-window.9
  11.2 2.4 %scatter_custom_fusion = s32[1024]{0:T(1024)S(1)} fusion(s32[512]{0:T(512)S(1)} %bitcast.95, s32[512]{0:T(512)S(1)} %add_select_fusion, s32[]{:T(128)} %constant.33.clone.1), kind=kCustom, calls=%fused_computation.53 | custom fusion | bytes 4100 | tf_op jit(solution)/shard_map/scatter | solution.py:67
  13.7 1.4 fusion.8
  15.1 1.4 fusion.10
  16.5 5.6 %gather_fusion = bf16[1024,1536]{1,0:T(8,128)(2,1)} fusion(bf16[257,1536]{1,0:T(8,128)(2,1)S(1)} %concatenate.3, s32[1024]{0:T(1024)S(1)} %fusion.23), kind=kCustom, calls=%fused_computation | custom fusion | bytes 6295552 | tf_op jit(solution)/shard_map/gather | solution.py:70
  22.1 1.2 constant_dynamic-slice_fusion
  23.3 26.4 %all_to_all.17 = bf16[4,256,384]{2,1,0:T(8,128)(2,1)} all-to-all(bf16[4,256,384]{2,1,0:T(8,128)(2,1)S(1)} %constant_dynamic-slice_fusion), channel_id=1, replica_groups=mesh['grp'=2,'ep'=4,'tp'=4] {'ep'}, dimensions={0} | all-to-all | bytes 1572864 | tf_op jit(solution)/shard_map/all_to_all | solution.py:78
  49.8 27.7 %all-gather.2.cloned.1.call-done = bf16[4,256,1536]{2,1,0:T(8,128)(2,1)} async-done(((bf16[4,256,384]{2,1,0:T(8,128)(2,1)}), bf16[4,256,1536]{2,1,0:T(8,128)(2,1)}) %all-gather.2.cloned.1.call-update) | async-done | bytes 3145744 | tf_op jit(solution)/shard_map/all_gather | solution.py:79
  77.5 5.4 %fusion.2 = f32[4,256,768]{2,1,0:T(8,128)S(1)} fusion(bf16[4,256,1536]{2,1,0:T(8,128)(2,1)} %all-gather.2.cloned.1.call-done, bf16[1,1536,768]{2,1,0:T(8,128)(2,1)} %param.22), kind=kOutput, calls=%fused_computation.7 | convolution fusion | flops 2415919104 | bytes 8650752 | tf_op jit(solution)/shard_map/scd,df->scf/dot_general | solution.py:81
  82.8 2.9 %multiply_convert_fusion = bf16[4,256,768]{2,1,0:T(8,128)(2,1)S(1)} fusion(f32[4,256,768]{2,1,0:T(8,128)S(1)} %fusion.2, bf16[4,256,1536]{2,1,0:T(8,128)(2,1)S(1)} %copy-done.8, bf16[1,1536,768]{2,1,0:T(8,128)(2,1)S(1)} %copy-done.9), kind=kOutput, calls=%fused_computation.5 | convolution fusion | flops 2420637696 | bytes 10223616 | tf_op jit(solution)/shard_map/scd,df->scf/dot_general | solution.py:80
  85.8 4.0 %fusion = bf16[1536,1024]{0,1:T(8,128)(2,1)} fusion(bf16[1024,768]{1,0:T(8,128)(2,1)S(1)} %bitcast.99, bf16[1,768,1536]{2,1,0:T(8,128)(2,1)S(1)} %copy-done), kind=kOutput, calls=%fused_computation.4 | convolution fusion | flops 2417491968 | bytes 7077888 | tf_op jit(solution)/shard_map/fd,sf->ds/dot_general | solution.py:85
  89.8 4.6 %copy.49 = bf16[1536,1024]{1,0:T(8,128)(2,1)} copy(bf16[1536,1024]{0,1:T(8,128)(2,1)} %fusion) | data formatting | bytes 6291456
  94.7 0.4 copy-done.4
  95.1 0.8 copy.43
  95.9 0.8 copy.47
  96.7 13.9 %all_gather.9 = bf16[512,256]{1,0:T(8,128)(2,1)S(1)} all-gather(bf16[128,256]{1,0:T(8,128)(2,1)S(1)} %copy-done.1), channel_id=1, replica_groups=mesh['grp'=2,'ep'=4,'tp'=4] {'ep'}, dimensions={0}, use_global_device_ids=true | all-gather | bytes 327680 | tf_op jit(solution)/shard_map/all_gather | solution.py:15
  110.9 1.3 fusion.30
  112.2 20.3 %reduce-scatter.4.cloned.1.call-done = bf16[384,1024]{1,0:T(8,128)(2,1)} async-done(((bf16[1536,1024]{1,0:T(8,128)(2,1)}), bf16[384,1024]{1,0:T(8,128)(2,1)}) %reduce-scatter.4.cloned.1.call-update) | async-done | bytes 786448
  132.5 2.3 %copy.50 = bf16[384,1024]{0,1:T(8,128)(2,1)} copy(bf16[384,1024]{1,0:T(8,128)(2,1)} %reduce-scatter.4.cloned.1.call-done) | data formatting | bytes 1572864
  134.8 4.7 %all-to-all-start.1 = ((bf16[384,4,256]{0,2,1:T(8,128)(2,1)}), bf16[384,4,256]{0,2,1:T(8,128)(2,1)S(1)}, u32[]{:S(2)}, u32[]{:S(2)}) async-start(bf16[384,4,256]{0,2,1:T(8,128)(2,1)} %bitcast.87), calls=%async_computation.1 | async-start | bytes 1572864 | tf_op jit(solution)/shard_map/all_to_all | solution.py:92
  139.5 27.2 %all_gather.10 = bf16[512,256]{1,0:T(8,128)(2,1)S(1)} all-gather(bf16[128,256]{1,0:T(8,128)(2,1)S(1)} %copy-done.2), channel_id=1, replica_groups=mesh['grp'=2,'ep'=4,'tp'=4] {'ep'}, dimensions={0}, use_global_device_ids=true | all-gather | bytes 327680 | tf_op jit(solution)/shard_map/all_gather | solution.py:16
  166.7 0.9 copy.38
  167.6 1.5 fusion.11
  169.1 1.7 convolution_divide_fusion
  171.1 0.7 copy.45
  171.8 1.9 %gather_fusion.1 = bf16[512,384]{1,0:T(8,128)(2,1)S(1)} fusion(bf16[384,1024]{0,1:T(8,128)(2,1)S(1)} %bitcast.85, s32[1024]{0:T(1024)S(1)} %pad_clamp_fusion), kind=kCustom, calls=%fused_computation.1 | custom fusion | bytes 788480 | tf_op jit(solution)/shard_map/jit(_take)/gather | solution.py:94
  173.9 1.7 fusion.15
  175.7 0.7 copy.55
  (47 shorter events, 1.8 us)
Async XLA Ops:
  7.2 78.6 %copy-start = (bf16[1,768,1536]{2,1,0:T(8,128)(2,1)S(1)}, bf16[1,768,1536]{2,1,0:T(8,128)(2,1)}, u32[]{:S(2)}) copy-start(bf16[1,768,1536]{2,1,0:T(8,128)(2,1)} %param.23) | copy-start | bytes 7077892
  7.2 70.3 %all-gather.2.cloned.1.call-start = ((), (), s32[]{:S(2)}) async-start(), calls=%async_computation.3 | async-start | bytes 3932160 | tf_op jit(solution)/shard_map/all_gather | solution.py:79
  49.7 82.8 %reduce-scatter.4.cloned.1.call-start = ((), (), s32[]{:S(2)}) async-start(), calls=%async_computation.4 | async-start | bytes 3932160
  77.4 5.4 %copy-start.8 = (bf16[4,256,1536]{2,1,0:T(8,128)(2,1)S(1)}, bf16[4,256,1536]{2,1,0:T(8,128)(2,1)}, u32[]{:S(2)}) copy-start(bf16[4,256,1536]{2,1,0:T(8,128)(2,1)} %all-gather.2.cloned.1.call-done) | copy-start | bytes 9437188
  77.4 5.4 %copy-start.9 = (bf16[1,1536,768]{2,1,0:T(8,128)(2,1)S(1)}, bf16[1,1536,768]{2,1,0:T(8,128)(2,1)}, u32[]{:S(2)}) copy-start(bf16[1,1536,768]{2,1,0:T(8,128)(2,1)} %param.21) | copy-start | bytes 7077892
  94.4 0.7 copy-start.4
  94.4 1.4 copy-start.5
  94.4 2.3 %copy-start.1 = (bf16[128,256]{1,0:T(8,128)(2,1)S(1)}, bf16[128,256]{1,0:T(8,128)(2,1)}, u32[]{:S(2)}) copy-start(bf16[128,256]{1,0:T(8,128)(2,1)} %param.13) | copy-start | bytes 196612
  94.4 16.4 %copy-start.3 = (bf16[128,256]{1,0:T(8,128)(2,1)S(1)}, bf16[128,256]{1,0:T(8,128)(2,1)}, u32[]{:S(2)}) copy-start(bf16[128,256]{1,0:T(8,128)(2,1)} %param.12) | copy-start | bytes 196612
  94.5 45.1 %copy-start.2 = (bf16[128,256]{1,0:T(8,128)(2,1)S(1)}, bf16[128,256]{1,0:T(8,128)(2,1)}, u32[]{:S(2)}) copy-start(bf16[128,256]{1,0:T(8,128)(2,1)} %param.14) | copy-start | bytes 196612
  112.2 58.6 %copy-start.6 = (f32[2]{0:T(128)S(1)}, f32[2]{0:T(128)}, u32[]{:S(2)}) copy-start(f32[2]{0:T(128)} %param.15) | copy-start | bytes 28
  134.8 36.2 %copy-start.7 = (f32[128]{0:T(128)S(1)}, f32[128]{0:T(128)}, u32[]{:S(2)}) copy-start(f32[128]{0:T(128)} %param.16) | copy-start | bytes 1540
  134.8 37.1 %all-to-all-start.1 = ((bf16[384,4,256]{0,2,1:T(8,128)(2,1)}), bf16[384,4,256]{0,2,1:T(8,128)(2,1)S(1)}, u32[]{:S(2)}, u32[]{:S(2)}) async-start(bf16[384,4,256]{0,2,1:T(8,128)(2,1)} %bitcast.87), calls=%async_computation.1 | async-start | bytes 1572864 | tf_op jit(solution)/shard_map/all_to_all | solution.py:92
Sparse Core Ops, SparseCore 0:
  49.8 27.5 all-gather.1
  94.6 37.8 reduce-scatter.3
where the time goes:
time: 184 us; the launch traced here: 183 us
  blocking collectives  67.5 us (37%)
  waiting for transfers between devices  48 us (26%)
  local copies, waits for them, and re-layouts  24.9 us (14%)
  matrix products  17 us (9%)
  between operations  14.3 us (8%)
  other arithmetic  6.72 us (4%)
  starting transfers between devices  4.81 us (3%)
    all_gather x1, waiting for transfers between devices, experts(): piece = lax.all_gather(arrived, 'tp', axis=2, tiled=True)  27.7 us
    all_gather x1, blocking collectives, attend(): value_piece = lax.all_gather(values, 'ep', axis=0, tiled=True)  27.2 us
    all_to_all x1, blocking collectives, experts(): lax.all_to_all(own_columns, 'ep', split_axis=0, concat_axis=0, tiled=True)  26.4 us
    unnamed x3, waiting for transfers between devices  20.3 us
    all_gather x1, blocking collectives, attend(): key_piece = lax.all_gather(keys, 'ep', axis=0, tiled=True)  13.9 us
    unnamed x26, local copies, waits for them, and re-layouts  10 us
    gather x1, local copies, waits for them, and re-layouts, experts(): outgoing = padded[owners].reshape(expert_count, capacity, width)  5.61 us
    dot_general x1, matrix products, experts(): jnp.einsum('scd,df->scf', piece, up_mat, preferred_element_type=jnp.float32)  5.36 us
  transfers between devices with their start and end apart: 3, of which 2 were waited for; matrix products, arithmetic and copies ran while one was open for 5% of the time, Pallas kernels for 0%

commit v1 on v0

--- a/solution.py
+++ b/solution.py
@@ -76,7 +76,9 @@
         outgoing, lax.axis_index("tp") * slice_width, slice_width, 2
     )
     arrived = lax.all_to_all(own_columns, "ep", split_axis=0, concat_axis=0, tiled=True)
-    piece = lax.all_gather(arrived, "tp", axis=2, tiled=True)
+    piece = jnp.concatenate(
+        lax.all_to_all(jnp.stack([arrived] * lax.axis_size("tp")), "tp", 0, 0), axis=2
+    )
     gate = jnp.einsum("scd,df->scf", piece, gate_mat, preferred_element_type=jnp.float32)
     upward = jnp.einsum("scd,df->scf", piece, up_mat, preferred_element_type=jnp.float32)
     hidden = (jax.nn.silu(gate) * upward).astype(jnp.bfloat16)

time: 184 us -> 193 us (1.049)
  blocking collectives: 67.5 us -> 107 us
  waiting for transfers between devices: 48 us -> 17.9 us
  matrix products: 17 us -> 14.3 us
  local copies, waits for them, and re-layouts: 24.9 us -> 27 us
    all_to_all x0 -> x1, blocking collectives: none -> 39.5 us  [experts(): lax.all_to_all(jnp.stack([arrived] * lax.axis_size('tp')), 'tp', 0, 0)]
    all_gather x1 -> x0, waiting for transfers between devices: 27.7 us -> none  [experts(): piece = lax.all_gather(arrived, 'tp', axis=2, tiled=True)]
    dot_general x1, matrix products: 5.36 us -> 2.59 us  [experts(): jnp.einsum('scd,df->scf', piece, up_mat, preferred_element_type=jnp.float32)]
    unnamed x3 -> x2, waiting for transfers between devices: 20.3 us -> 17.9 us
  transfers between devices with their start and end apart: 3 -> 2, of which waited for: 2 -> 1; matrix products, arithmetic and copies ran while one was open for 5% -> 4% of each run, Pallas kernels for 0% -> 0%
where the time goes in v1:
time: 193 us; the launch traced here: 192 us
  blocking collectives  107 us (55%)
  local copies, waits for them, and re-layouts  27 us (14%)
  waiting for transfers between devices  17.9 us (9%)
  matrix products  14.3 us (7%)
  between operations  14.3 us (7%)
  other arithmetic  6.72 us (3%)
  starting transfers between devices  4.78 us (2%)
    all_to_all x1, blocking collectives, experts(): lax.all_to_all(jnp.stack([arrived] * lax.axis_size('tp')), 'tp', 0, 0)  39.5 us
    all_gather x1, blocking collectives, attend(): value_piece = lax.all_gather(values, 'ep', axis=0, tiled=True)  27.2 us
    all_to_all x1, blocking collectives, experts(): lax.all_to_all(own_columns, 'ep', split_axis=0, concat_axis=0, tiled=True)  26.3 us
    unnamed x2, waiting for transfers between devices  17.9 us
    all_gather x1, blocking collectives, attend(): key_piece = lax.all_gather(keys, 'ep', axis=0, tiled=True)  14.4 us
    unnamed x26, local copies, waits for them, and re-layouts  11.3 us
    gather x1, local copies, waits for them, and re-layouts, experts(): outgoing = padded[owners].reshape(expert_count, capacity, width)  5.61 us
    all_to_all x1, starting transfers between devices, experts(): back = lax.all_to_all(summed, 'ep', split_axis=1, concat_axis=1, tiled=True)  4.74 us
  transfers between devices with their start and end apart: 2, of which 1 were waited for; matrix products, arithmetic and copies ran while one was open for 4% of the time, Pallas kernels for 0%

profile of v1, /device:TPU:0, one launch (start us, length us, event | category | flops | bytes accessed | tf_op | source)
XLA Modules:
  0.0 192.3 jit_solution(18257608637831585549)
XLA Ops:
  7.2 1.0 copy.41
  8.5 0.7 broadcast_multiply_fusion
  9.2 1.2 reduce-window.6
  11.2 2.4 %scatter_custom_fusion = s32[1024]{0:T(1024)S(1)} fusion(s32[512]{0:T(512)S(1)} %bitcast.101, s32[512]{0:T(512)S(1)} %add_select_fusion, s32[]{:T(128)} %constant.33.clone.1), kind=kCustom, calls=%fused_computation.53 | custom fusion | bytes 4100 | tf_op jit(solution)/shard_map/scatter | solution.py:67
  13.7 1.4 fusion.8
  15.1 1.4 fusion.10
  16.5 5.6 %gather_fusion = bf16[1024,1536]{1,0:T(8,128)(2,1)} fusion(bf16[257,1536]{1,0:T(8,128)(2,1)S(1)} %concatenate.3, s32[1024]{0:T(1024)S(1)} %fusion.23), kind=kCustom, calls=%fused_computation | custom fusion | bytes 6295552 | tf_op jit(solution)/shard_map/gather | solution.py:70
  22.1 1.2 constant_dynamic-slice_fusion
  23.3 26.3 %all_to_all.22 = bf16[4,256,384]{2,1,0:T(8,128)(2,1)S(1)} all-to-all(bf16[4,256,384]{2,1,0:T(8,128)(2,1)S(1)} %constant_dynamic-slice_fusion), channel_id=1, replica_groups=mesh['grp'=2,'ep'=4,'tp'=4] {'ep'}, dimensions={0} | all-to-all | bytes 1572864 | tf_op jit(solution)/shard_map/all_to_all | solution.py:78
  49.6 0.4 stack.2
  50.0 39.5 %all_to_all.23 = bf16[4,4,256,384]{3,2,1,0:T(8,128)(2,1)S(1)} all-to-all(bf16[4,4,256,384]{3,2,1,0:T(8,128)(2,1)S(1)} %stack.2), channel_id=1, replica_groups=mesh['grp'=2,'ep'=4,'tp'=4] {'tp'}, dimensions={0} | all-to-all | bytes 6291456 | tf_op jit(solution)/shard_map/all_to_all | solution.py:80
  89.9 1.3 copy-done.8
  91.1 2.6 %fusion.2 = f32[4,256,768]{2,1,0:T(8,128)S(1)} fusion(bf16[4,256,1536]{2,1,0:T(8,128)(2,1)S(1)} %bitcast.91, bf16[1,1536,768]{2,1,0:T(8,128)(2,1)S(1)} %copy-done.8), kind=kOutput, calls=%fused_computation.7 | convolution fusion | flops 2415919104 | bytes 8650752 | tf_op jit(solution)/shard_map/scd,df->scf/dot_general | solution.py:83
  93.8 2.9 %multiply_convert_fusion = bf16[4,256,768]{2,1,0:T(8,128)(2,1)S(1)} fusion(f32[4,256,768]{2,1,0:T(8,128)S(1)} %fusion.2, bf16[4,256,1536]{2,1,0:T(8,128)(2,1)S(1)} %bitcast.92, bf16[1,1536,768]{2,1,0:T(8,128)(2,1)S(1)} %copy-done.9), kind=kOutput, calls=%fused_computation.5 | convolution fusion | flops 2420637696 | bytes 10223616 | tf_op jit(solution)/shard_map/scd,df->scf/dot_general | solution.py:82
  96.7 4.0 %fusion = bf16[1536,1024]{0,1:T(8,128)(2,1)} fusion(bf16[1024,768]{1,0:T(8,128)(2,1)S(1)} %bitcast.105, bf16[1,768,1536]{2,1,0:T(8,128)(2,1)S(1)} %copy-done), kind=kOutput, calls=%fused_computation.4 | convolution fusion | flops 2417491968 | bytes 7077888 | tf_op jit(solution)/shard_map/fd,sf->ds/dot_general | solution.py:87
  100.7 4.6 %copy.51 = bf16[1536,1024]{1,0:T(8,128)(2,1)} copy(bf16[1536,1024]{0,1:T(8,128)(2,1)} %fusion) | data formatting | bytes 6291456
  105.6 0.4 copy-done.4
  106.0 0.8 copy.44
  106.8 0.8 copy.49
  107.6 14.4 %all_gather.6 = bf16[512,256]{1,0:T(8,128)(2,1)S(1)} all-gather(bf16[128,256]{1,0:T(8,128)(2,1)S(1)} %copy-done.1), channel_id=1, replica_groups=mesh['grp'=2,'ep'=4,'tp'=4] {'ep'}, dimensions={0}, use_global_device_ids=true | all-gather | bytes 327680 | tf_op jit(solution)/shard_map/all_gather | solution.py:15
  122.3 1.3 fusion.30
  123.7 17.9 %reduce-scatter.4.cloned.1.call-done = bf16[384,1024]{1,0:T(8,128)(2,1)} async-done(((bf16[1536,1024]{1,0:T(8,128)(2,1)}), bf16[384,1024]{1,0:T(8,128)(2,1)}) %reduce-scatter.4.cloned.1.call-update) | async-done | bytes 786448
  141.6 2.3 %copy.52 = bf16[384,1024]{0,1:T(8,128)(2,1)} copy(bf16[384,1024]{1,0:T(8,128)(2,1)} %reduce-scatter.4.cloned.1.call-done) | data formatting | bytes 1572864
  143.9 4.7 %all-to-all-start.2 = ((bf16[384,4,256]{0,2,1:T(8,128)(2,1)}), bf16[384,4,256]{0,2,1:T(8,128)(2,1)S(1)}, u32[]{:S(2)}, u32[]{:S(2)}) async-start(bf16[384,4,256]{0,2,1:T(8,128)(2,1)} %bitcast.93), calls=%async_computation.2 | async-start | bytes 1572864 | tf_op jit(solution)/shard_map/all_to_all | solution.py:94
  148.6 27.2 %all_gather.7 = bf16[512,256]{1,0:T(8,128)(2,1)S(1)} all-gather(bf16[128,256]{1,0:T(8,128)(2,1)S(1)} %copy-done.2), channel_id=1, replica_groups=mesh['grp'=2,'ep'=4,'tp'=4] {'ep'}, dimensions={0}, use_global_device_ids=true | all-gather | bytes 327680 | tf_op jit(solution)/shard_map/all_gather | solution.py:16
  175.8 0.9 copy.39
  176.7 1.5 fusion.11
  178.2 1.7 convolution_divide_fusion
  180.2 0.7 copy.47
  180.9 1.9 %gather_fusion.1 = bf16[512,384]{1,0:T(8,128)(2,1)S(1)} fusion(bf16[384,1024]{0,1:T(8,128)(2,1)S(1)} %bitcast.88, s32[1024]{0:T(1024)S(1)} %pad_clamp_fusion), kind=kCustom, calls=%fused_computation.1 | custom fusion | bytes 788480 | tf_op jit(solution)/shard_map/jit(_take)/gather | solution.py:96
  183.0 1.7 fusion.15
  184.8 0.7 copy.58
  (47 shorter events, 2.5 us)
Async XLA Ops:
  7.2 89.5 %copy-start = (bf16[1,768,1536]{2,1,0:T(8,128)(2,1)S(1)}, bf16[1,768,1536]{2,1,0:T(8,128)(2,1)}, u32[]{:S(2)}) copy-start(bf16[1,768,1536]{2,1,0:T(8,128)(2,1)} %param.23) | copy-start | bytes 7077892
  7.2 134.4 %reduce-scatter.4.cloned.1.call-start = ((), (), s32[]{:S(2)}) async-start(), calls=%async_computation.4 | async-start | bytes 3932160
  89.5 1.7 copy-start.8
  91.1 2.6 %copy-start.9 = (bf16[1,1536,768]{2,1,0:T(8,128)(2,1)S(1)}, bf16[1,1536,768]{2,1,0:T(8,128)(2,1)}, u32[]{:S(2)}) copy-start(bf16[1,1536,768]{2,1,0:T(8,128)(2,1)} %param.21) | copy-start | bytes 7077892
  105.3 0.7 copy-start.4
  105.3 1.4 copy-start.5
  105.3 2.3 %copy-start.1 = (bf16[128,256]{1,0:T(8,128)(2,1)S(1)}, bf16[128,256]{1,0:T(8,128)(2,1)}, u32[]{:S(2)}) copy-start(bf16[128,256]{1,0:T(8,128)(2,1)} %param.13) | copy-start | bytes 196612
  105.3 16.9 %copy-start.3 = (bf16[128,256]{1,0:T(8,128)(2,1)S(1)}, bf16[128,256]{1,0:T(8,128)(2,1)}, u32[]{:S(2)}) copy-start(bf16[128,256]{1,0:T(8,128)(2,1)} %param.12) | copy-start | bytes 196612
  105.4 43.2 %copy-start.2 = (bf16[128,256]{1,0:T(8,128)(2,1)S(1)}, bf16[128,256]{1,0:T(8,128)(2,1)}, u32[]{:S(2)}) copy-start(bf16[128,256]{1,0:T(8,128)(2,1)} %param.14) | copy-start | bytes 196612
  123.7 56.3 %copy-start.6 = (f32[2]{0:T(128)S(1)}, f32[2]{0:T(128)}, u32[]{:S(2)}) copy-start(f32[2]{0:T(128)} %param.15) | copy-start | bytes 28
  143.9 36.2 %copy-start.7 = (f32[128]{0:T(128)S(1)}, f32[128]{0:T(128)}, u32[]{:S(2)}) copy-start(f32[128]{0:T(128)} %param.16) | copy-start | bytes 1540
  143.9 37.1 %all-to-all-start.2 = ((bf16[384,4,256]{0,2,1:T(8,128)(2,1)}), bf16[384,4,256]{0,2,1:T(8,128)(2,1)S(1)}, u32[]{:S(2)}, u32[]{:S(2)}) async-start(bf16[384,4,256]{0,2,1:T(8,128)(2,1)} %bitcast.93), calls=%async_computation.2 | async-start | bytes 1572864 | tf_op jit(solution)/shard_map/all_to_all | solution.py:94
Sparse Core Ops, SparseCore 0:
  105.5 36.0 reduce-scatter.3
